TPU v7x, 32 devices: a whole 2x2x4 slice. The times are simulated.
32 devices in a mesh: kv: 16 (over z, y, x), tp: 2 (over core).
Axes of the slice: x: 2, y: 2, z: 4, core: 2. Of those that a mesh axis runs over, the one named last changes fastest.
Arguments:
- tokens: bfloat16 [256, 2048], P('kv', 'tp'), may hold values from -20 to 20
- norm_gain: float32 [2048], replicated, may hold values from 0.1 to 1.9
- w_query: bfloat16 [2048, 1024], P(None, 'tp'), may hold values from -0.125 to 0.125
- w_key: bfloat16 [2048, 1024], P(None, 'tp'), may hold values from -0.125 to 0.125
- w_value: bfloat16 [2048, 1024], P(None, 'tp'), may hold values from -0.125 to 0.125
- w_outgate: bfloat16 [2048, 1024], P(None, 'tp'), may hold values from -0.125 to 0.125
- w_input_gate: bfloat16 [2048, 8], replicated, may hold values from -0.125 to 0.125
- w_forget_gate: bfloat16 [2048, 8], replicated, may hold values from -0.125 to 0.125
- memory: float32 [256, 8, 128, 128], P('kv', 'tp'), may hold values from -6 to 6
- normalizer: float32 [256, 8, 128], P('kv', 'tp'), may hold values from -6 to 6
- memory_max: float32 [256, 8], P('kv', 'tp'), may hold values from -2 to 300
- w_output: bfloat16 [1024, 2048], P(None, 'tp'), may hold values from -0.1875 to 0.1875
- ffn_gain: float32 [2048], P('tp'), may hold values from 0.1 to 1.9
- w_gate: bfloat16 [2048, 5632], P('tp', 'kv'), may hold values from -0.125 to 0.125
- w_up: bfloat16 [2048, 5632], P('tp', 'kv'), may hold values from -0.125 to 0.125
- w_down: bfloat16 [5632, 2048], P('kv', 'tp'), may hold values from -0.078125 to 0.078125
Outputs:
- result: bfloat16 [256, 2048], P('kv', 'tp')
- new_memory: float32 [256, 8, 128, 128], P('kv', 'tp')
- new_normalizer: float32 [256, 8, 128], P('kv', 'tp')
- new_max: float32 [256, 8], P('kv', 'tp')
All inputs are finite; a program needn't handle non-finite values.
Results may differ from a plain program's by a relative error of at most 0.013.
Values may be sent and summed in bfloat16 or wider, within the bound.
A program may use at most 64 MiB of HBM per device.

v0:
```python
import functools

import jax
import jax.numpy as jnp
from jax import lax
from jax.experimental import pallas as pl
from jax.experimental.pallas import tpu as pltpu
from jax.sharding import PartitionSpec as P

F32, BF16 = jnp.float32, jnp.bfloat16
MESH = pl.DeviceIdType.MESH
ANY = pl.BlockSpec(memory_space=pl.ANY)
VMEM = pl.BlockSpec(memory_space=pltpu.VMEM)
DEPTH = 4


def partner(index, bits):
    out, bit = index, 1
    while bit <= bits:
        if bits & bit:
            out = out + bit - 2 * bit * ((index // bit) % 2)
        bit *= 2
    return out


def split_groups(count):
    slow = 1
    while slow * slow < count:
        slow *= 2
    assert count % slow == 0
    return slow, count // slow


def greet(devices):
    barrier = pltpu.get_barrier_semaphore()
    for device in devices:
        pl.semaphore_signal(barrier, inc=1, device_id=device, device_id_type=MESH)
    pl.semaphore_wait(barrier, len(devices))


def nt_dot(a, b):
    return lax.dot_general(a, b, (((1,), (1,)), ((), ())), preferred_element_type=F32)


def step_kernel(
    nz, ny, nt, width,
    tokens_ref, norm_gain_ref, w_ig_ref, w_fg_ref, normalizer_ref, memory_max_ref, gain_ref,
    w_key_hbm, w_value_hbm, w_query_hbm, w_outgate_hbm, memory_hbm, w_out_hbm, w_gate_hbm, w_up_hbm, w_down_hbm,
    out_ref, aux_ref, new_max_ref,
    w_key, w_value, w_query, w_outgate, memory, w_out, w_gate, w_up, w_down,
    tok, normed, num, mixed_ref, mix, rows, part, part_in, down, down_in, total, total_in,
    load_sem, tok_sem, mix_sem, zed_sem, plane_sem, part_sem, down_sem, total_sem,
):
    k, t = lax.axis_index("kv"), lax.axis_index("tp")
    z, y = k // ny, k % ny
    own, cols = rows.shape[1], rows.shape[2]
    heads, dim = memory.shape[0], memory.shape[3]
    ff = w_down.shape[0]
    pad = (part.shape[2] - 128) // 2

    pairs = [(w_key_hbm, w_key), (w_value_hbm, w_value), (w_query_hbm, w_query), (w_outgate_hbm, w_outgate)]
    pairs += [(memory_hbm.at[:, h], memory.at[h]) for h in range(heads)]
    pairs += [(w_out_hbm, w_out), (w_gate_hbm, w_gate), (w_up_hbm, w_up), (w_down_hbm, w_down)]
    loads = [pltpu.make_async_copy(src, dst, load_sem.at[i]) for i, (src, dst) in enumerate(pairs)]
    for load in loads[:DEPTH]:
        load.start()

    def arrived(i):
        loads[i].wait()
        if i + DEPTH < len(loads):
            loads[i + DEPTH].start()

    def at_zed(off):
        return (partner(z, off) * ny + y, t)

    def at_plane(off):
        return (z * ny + partner(y, off), t)

    def at_tp(off):
        return (k, partner(t, off))

    greet(
        [at_tp(o) for o in range(1, nt)]
        + [at_plane(o) for o in range(1, ny)]
        + [at_zed(o) for o in range(1, nz)]
    )
    started = []

    def send(src, dst, sems, device):
        copy = pltpu.make_async_remote_copy(
            src_ref=src, dst_ref=dst, send_sem=sems.at[0], recv_sem=sems.at[1],
            device_id=device, device_id_type=MESH,
        )
        copy.start()
        started.append(copy)
        return copy

    toks = [send(tokens_ref, tok.at[o - 1], tok_sem.at[o - 1], at_tp(o)) for o in range(1, nt)]
    blocks = [(t, tokens_ref[...].astype(F32))]
    for o in range(1, nt):
        toks[o - 1].wait_recv()
        blocks.append((partner(t, o), tok[o - 1].astype(F32)))
    square = blocks[0][1] * blocks[0][1]
    square = jnp.sum(square, axis=-1, keepdims=True)
    for _, block in blocks[1:]:
        square = square + jnp.sum(block * block, axis=-1, keepdims=True)
    row_scale = lax.rsqrt(square / width + 1e-06)
    for owner, block in blocks:
        at = pl.ds(pl.multiple_of(owner * cols, cols), cols)
        normed[:, at] = (block * row_scale * norm_gain_ref[:, at]).astype(BF16)
    x = normed[...]
    igates, fgates = nt_dot(x, w_ig_ref[...]), nt_dot(x, w_fg_ref[...])

    def projected(i, weight):
        arrived(i)
        return jnp.dot(x, weight[...], preferred_element_type=F32)

    keys = projected(0, w_key)
    values = projected(1, w_value)
    queries = projected(2, w_query) * dim ** (-0.5)
    outgates = projected(3, w_outgate)
    lane = lax.broadcasted_iota(jnp.int32, igates.shape, 1)
    diagonal = lax.broadcasted_iota(jnp.int32, (own, own), 0) == lax.broadcasted_iota(jnp.int32, (own, own), 1)
    for h in range(heads):
        mine = lane == t * heads + h
        igate = jnp.sum(jnp.where(mine, igates, 0.0), axis=-1, keepdims=True)
        forget = jnp.sum(jnp.where(mine, fgates, 0.0), axis=-1, keepdims=True)
        carried = jnp.minimum(forget, 0.0) - jnp.log1p(jnp.exp(-jnp.abs(forget)))
        carried = carried + jnp.sum(jnp.where(diagonal, memory_max_ref[h : h + 1, :], 0.0), axis=-1, keepdims=True)
        new_max = jnp.maximum(carried, igate)
        keep_weight = jnp.exp(carried - new_max)
        new_max_ref[h : h + 1, :] = jnp.sum(jnp.where(diagonal, new_max, 0.0), axis=0, keepdims=True)
        at = slice(h * dim, (h + 1) * dim)
        key, value, query = jnp.exp(igate - new_max) * keys[:, at], values[:, at], queries[:, at]
        keep_wide = jnp.broadcast_to(keep_weight, key.shape)
        aux_ref[0, h], aux_ref[1, h], aux_ref[2, h] = keep_wide, key, value
        denominator = jnp.sum(query * (keep_wide * normalizer_ref[:, h, :] + key), axis=-1, keepdims=True)
        match = jnp.sum(query * key, axis=-1, keepdims=True)
        turned = query.T
        arrived(4 + h)
        for r in range(own):
            num[r : r + 1, :] = jnp.sum(memory[h, r] * turned[:, r : r + 1], axis=0, keepdims=True)
        numerator = keep_wide * num[...] + match * value
        cell_out = numerator / jnp.maximum(jnp.abs(denominator), jnp.exp(-new_max))
        centered = cell_out - jnp.mean(cell_out, axis=-1, keepdims=True)
        head_var = jnp.mean(centered * centered, axis=-1, keepdims=True)
        gate = 1.0 / (1.0 + jnp.exp(-outgates[:, at]))
        mixed_ref[:, at] = (gate * centered * lax.rsqrt(head_var + 1e-05)).astype(BF16)

    mixes = [send(mixed_ref, mix.at[o - 1], mix_sem.at[o - 1], at_tp(o)) for o in range(1, nt)]
    first = 4 + heads
    arrived(first)
    inner = mixed_ref.shape[1]

    def project(value, owner):
        return jnp.dot(value, w_out[pl.ds(pl.multiple_of(owner * inner, inner), inner), :], preferred_element_type=F32)

    acc = tokens_ref[...].astype(F32) + project(mixed_ref[...], t)
    for o in range(1, nt):
        mixes[o - 1].wait_recv()
        acc = acc + project(mix[o - 1], partner(t, o))
    rows[k] = acc.astype(BF16)

    zeds = {o: send(rows.at[k], rows.at[k], zed_sem.at[o], at_zed(o)) for o in range(1, nz)}
    planes = {}

    def spread(off):
        source = partner(z, off) * ny + y
        if off:
            zeds[off].wait_recv()
        for o in range(1, ny):
            planes[off, o] = send(rows.at[source], rows.at[source], plane_sem.at[off, o], at_plane(o))

    parts, gates, downs, totals, keep = {}, {}, {}, {}, {}

    def stage_a(off):
        for o in range(1, ny):
            planes[off, o].wait_recv()
        if off == 0:
            arrived(first + 1)
            arrived(first + 2)
        x = rows[pl.ds(partner(z, off) * ny, ny)].reshape(ny * own, cols)
        xf = x.astype(F32)
        square = jnp.sum(xf * xf, axis=-1, keepdims=True)
        h = (xf * gain_ref[...]).astype(BF16)
        gate = nt_dot(h, w_gate[...])
        up = nt_dot(h, w_up[...])
        high = square.astype(BF16).astype(F32)
        lane = lax.broadcasted_iota(jnp.int32, (ny * own, 128), 1)
        part[off, :, 0:ff] = gate.astype(BF16)
        part[off, :, pad : pad + ff] = up.astype(BF16)
        part[off, :, 2 * pad :] = jnp.where(lane < 64, high, square - high).astype(BF16)
        for o in range(1, nt):
            parts[off, o] = send(part.at[off], part_in.at[off, o - 1], part_sem.at[off, o - 1], at_tp(o))
        gates[off] = (gate, up, square)

    def stage_b(off):
        gate, up, square = gates.pop(off)
        for o in range(1, nt):
            parts[off, o].wait_recv()
            gate = gate + part_in[off, o - 1, :, 0:ff].astype(F32)
            up = up + part_in[off, o - 1, :, pad : pad + ff].astype(F32)
            tail = part_in[off, o - 1, :, 2 * pad :].astype(F32)
            square = square + jnp.sum(tail, axis=-1, keepdims=True) * (1.0 / 64)
        scale = lax.rsqrt(square / width + 1e-06)
        g = scale * gate
        hidden = (g / (1.0 + jnp.exp(-g)) * (scale * up)).astype(BF16)
        if off == min(1, nz - 1):
            arrived(first + 3)
        out = jnp.dot(hidden, w_down[...], preferred_element_type=F32)
        down[off] = out.reshape(ny, own, cols).astype(BF16)
        for o in range(1, ny):
            downs[off, o] = send(down.at[off, partner(y, o)], down_in.at[off, o - 1], down_sem.at[off, o], at_plane(o))

    def stage_c(off):
        acc = down[off, y].astype(F32)
        for o in range(1, ny):
            downs[off, o].wait_recv()
            acc = acc + down_in[off, o - 1].astype(F32)
        if off == 0:
            keep[0] = acc
        else:
            total[off] = acc.astype(BF16)
            totals[off] = send(total.at[off], total_in.at[off], total_sem.at[off], at_zed(off))

    spread(0)
    if nz > 1:
        spread(1)
    stage_a(0)
    for o in range(2, nz):
        spread(o)
    for o in range(1, nz + 1):
        if o < nz:
            stage_a(o)
        if o > 1:
            stage_b(o - 1)
        if o > 2:
            stage_c(o - 2)
    stage_b(0)
    if nz > 1:
        stage_c(nz - 1)
    stage_c(0)
    acc = rows[k].astype(F32) + keep[0]
    for o in range(1, nz):
        totals[o].wait_recv()
        acc = acc + total_in[o].astype(F32)
    out_ref[...] = acc.astype(BF16)
    for copy in started:
        copy.wait_send()


def update_kernel(chunk, memory_hbm, aux_ref, normalizer_ref, new_max_in, result_in, new_memory_hbm, new_norm_ref, new_max_ref, result_ref, memory, in_sem, out_sem):
    rows, heads = memory.shape[0], memory.shape[1]
    steps = range(rows // chunk)
    at = [pl.ds(i * chunk, chunk) for i in steps]
    loads = [pltpu.make_async_copy(memory_hbm.at[at[i]], memory.at[at[i]], in_sem.at[i]) for i in steps]
    stores = [pltpu.make_async_copy(memory.at[at[i]], new_memory_hbm.at[at[i]], out_sem.at[i]) for i in steps]
    for load in loads:
        load.start()
    turned = []
    for h in range(heads):
        new_norm_ref[:, h, :] = aux_ref[0, h] * normalizer_ref[:, h, :] + aux_ref[1, h]
        turned.append(aux_ref[1, h].T)
    new_max_ref[...] = new_max_in[...]
    result_ref[...] = result_in[...]
    for i in steps:
        loads[i].wait()
        for r in range(i * chunk, (i + 1) * chunk):
            for h in range(heads):
                memory[r, h] = aux_ref[0, h, r : r + 1, :] * memory[r, h] + turned[h][:, r : r + 1] * aux_ref[2, h, r : r + 1, :]
        stores[i].start()
    for store in stores:
        store.wait()


def per_device(
    mesh, tokens, norm_gain, w_query, w_key, w_value, w_outgate, w_input_gate, w_forget_gate,
    memory, normalizer, memory_max, w_output, ffn_gain, w_gate, w_up, w_down,
):
    n, nt = mesh.shape["kv"], mesh.shape["tp"]
    nz, ny = split_groups(n)
    own, cols = tokens.shape
    heads, dim = memory.shape[1], memory.shape[2]
    inner = heads * dim
    ff = w_down.shape[0]
    pad = -(-ff // 128) * 128
    dma = pltpu.SemaphoreType.DMA
    peers = max(nt - 1, 1)
    w_gate, w_up = w_gate.T, w_up.T
    vm = lambda like: pltpu.VMEM(like.shape, like.dtype)
    result, aux, new_max = pl.pallas_call(
        functools.partial(step_kernel, nz, ny, nt, cols * nt),
        out_shape=(
            jax.ShapeDtypeStruct((own, cols), BF16),
            jax.ShapeDtypeStruct((3, heads, own, dim), F32),
            jax.ShapeDtypeStruct((heads, own), F32),
        ),
        in_specs=[VMEM] * 7 + [ANY] * 9,
        out_specs=(VMEM, VMEM, VMEM),
        scratch_shapes=[
            vm(w_key), vm(w_value), vm(w_query), vm(w_outgate),
            pltpu.VMEM((heads, own, dim, dim), F32),
            vm(w_output), vm(w_gate), vm(w_up), vm(w_down),
            pltpu.VMEM((peers, own, cols), BF16),
            pltpu.VMEM((own, cols * nt), BF16),
            pltpu.VMEM((own, dim), F32),
            pltpu.VMEM((own, inner), BF16),
            pltpu.VMEM((peers, own, inner), BF16),
            pltpu.VMEM((n, own, cols), BF16),
            pltpu.VMEM((nz, ny * own, 2 * pad + 128), BF16),
            pltpu.VMEM((nz, peers, ny * own, 2 * pad + 128), BF16),
            pltpu.VMEM((nz, ny, own, cols), BF16),
            pltpu.VMEM((nz, ny, own, cols), BF16),
            pltpu.VMEM((nz, own, cols), BF16),
            pltpu.VMEM((nz, own, cols), BF16),
            dma((8 + heads,)),
            dma((peers, 2)),
            dma((peers, 2)),
            dma((nz, 2)),
            dma((nz, ny, 2)),
            dma((nz, peers, 2)),
            dma((nz, ny, 2)),
            dma((nz, 2)),
        ],
        compiler_params=pltpu.CompilerParams(collective_id=0, has_side_effects=True),
        name="decode_step",
    )(
        tokens, norm_gain.reshape(1, -1), w_input_gate.T, w_forget_gate.T, normalizer, memory_max.T,
        ffn_gain.reshape(1, cols), w_key, w_value, w_query, w_outgate, memory, w_output, w_gate, w_up, w_down,
    )
    chunk = 2 if own % 2 == 0 else 1
    new_memory, new_normalizer, new_max, result = pl.pallas_call(
        functools.partial(update_kernel, chunk),
        out_shape=(
            jax.ShapeDtypeStruct(memory.shape, F32),
            jax.ShapeDtypeStruct(normalizer.shape, F32),
            jax.ShapeDtypeStruct((heads, own), F32),
            jax.ShapeDtypeStruct(tokens.shape, BF16),
        ),
        in_specs=[ANY, VMEM, VMEM, VMEM, VMEM],
        out_specs=(ANY, VMEM, VMEM, VMEM),
        scratch_shapes=[vm(memory), dma((own // chunk,)), dma((own // chunk,))],
        name="memory_update",
    )(memory, aux, normalizer, new_max, result)
    return (result, new_memory, new_normalizer, new_max.T)


def solution(mesh):
    placed = (
        P("kv", "tp"),
        P(),
        P(None, "tp"),
        P(None, "tp"),
        P(None, "tp"),
        P(None, "tp"),
        P(),
        P(),
        P("kv", "tp", None, None),
        P("kv", "tp", None),
        P("kv", "tp"),
        P(None, "tp"),
        P("tp"),
        P("tp", "kv"),
        P("tp", "kv"),
        P("kv", "tp"),
    )
    return jax.shard_map(
        functools.partial(per_device, mesh),
        mesh=mesh,
        in_specs=placed,
        out_specs=(P("kv", "tp"), P("kv", "tp", None, None), P("kv", "tp", None), P("kv", "tp")),
        check_vma=False,
    )
```

profile of v0, /device:TPU:0, one launch (start us, length us, event | category | flops | bytes accessed | tf_op | source)
XLA Modules:
  0.0 41.8 jit_solution(13388604215299061388)
XLA Ops:
  0.6 36.0 %decode_step.1 = (bf16[16,1024]{1,0:T(8,128)(2,1)}, f32[3,4,16,128]{3,2,1,0:T(8,128)}, f32[4,16]{1,0:T(4,128)}) custom-call(bf16[16,1024]{1,0:T(8,128)(2,1)} %tokens_ref.1, f32[1,2048]{1,0:T(1,128)} %bitcast.12, bf16[8,2048]{1,0:T(8,128)(2,1)} %bitcast.10, bf16[8,2048]{1,0:T(8,128)(2,1)} %bitcast.11, f32[16,4,128]{2,1,0:T(4,128)} %normalizer_ref.3, ...), custom_call_target="tpu_custom_call" | custom-call | tf_op jit(solution)/shard_map/decode_step/pallas_call | solution.py:291
  36.6 5.2 %memory_update.1 = (f32[16,4,128,128]{3,2,1,0:T(8,128)}, f32[16,4,128]{2,1,0:T(4,128)}, f32[4,16]{1,0:T(4,128)}, bf16[16,1024]{1,0:T(8,128)(2,1)}) custom-call(f32[16,4,128,128]{3,2,1,0:T(8,128)} %memory_hbm.3, f32[3,4,16,128]{3,2,1,0:T(8,128)} %get-tuple-element.11.aux_ref, f32[16,4,128]{2,1,0:T(4,128)} %normalizer_ref.3, ...), custom_call_target="tpu_custom_call" | custom-call | tf_op jit(solution)/shard_map/memory_update/pallas_call | solution.py:332
where the time goes:
time: 42 us; the launch traced here: 41.8 us
  Pallas kernels  41.2 us (98%)
  between operations  0.64 us (2%)
    pallas_call x1, Pallas kernels, per_device(): pl.pallas_call(functools.partial(step_kernel, nz, ny, nt, cols * nt), out...  36 us
    pallas_call x1, Pallas kernels, per_device(): pl.pallas_call(functools.partial(update_kernel, chunk), out_shape=(jax.Sh...  5.2 us

commit v1 on v0

v1 whole, which is shorter than its diff:
```python
import functools

import jax
import jax.numpy as jnp
from jax import lax
from jax.experimental import pallas as pl
from jax.experimental.pallas import tpu as pltpu
from jax.sharding import PartitionSpec as P

F32, BF16 = jnp.float32, jnp.bfloat16
MESH = pl.DeviceIdType.MESH
ANY = pl.BlockSpec(memory_space=pl.ANY)
VMEM = pl.BlockSpec(memory_space=pltpu.VMEM)
HBM = pl.BlockSpec(memory_space=pltpu.HBM)
DEPTH = 6
VMEM_BYTES = 67043328


def partner(index, bits):
    out, bit = index, 1
    while bit <= bits:
        if bits & bit:
            out = out + bit - 2 * bit * ((index // bit) % 2)
        bit *= 2
    return out


def split_groups(count):
    slow = 1
    while slow * slow < count:
        slow *= 2
    assert count % slow == 0
    return slow, count // slow


def nt_dot(a, b):
    return lax.dot_general(a, b, (((1,), (1,)), ((), ())), preferred_element_type=F32)


def step_kernel(
    nz, ny, nt, width,
    tokens_hbm, norm_gain_hbm, w_ig_hbm, w_fg_hbm, normalizer_hbm, memory_max_hbm, gain_hbm,
    w_key_hbm, w_value_hbm, w_query_hbm, w_outgate_hbm, memory_hbm, w_out_hbm, w_gate_hbm, w_up_hbm, w_down_hbm,
    out_ref, memory, new_norm, new_max_ref,
    tokens_ref, norm_gain_ref, w_ig_ref, w_fg_ref, normalizer_ref, memory_max_ref, gain_ref,
    w_key, w_value, w_query, w_outgate, w_out, w_gate, w_up, w_down,
    tok, normed, num, factors, mixed_ref, mix, rows, part, part_in, down, down_in, total, total_in, ours,
    small_sem, load_sem, tok_sem, mix_sem, zed_recv, plane_recv, gather_send,
    part_recv, part_send, down_recv, total_recv, reduce_send,
):
    k, t = lax.axis_index("kv"), lax.axis_index("tp")
    z, y = k // ny, k % ny
    n, own, cols = rows.shape
    heads, dim = memory.shape[1], memory.shape[3]
    ff = w_down.shape[0]
    pad = (part.shape[2] - 128) // 2

    def at_zed(off):
        return (partner(z, off) * ny + y, t)

    def at_plane(off):
        return (z * ny + partner(y, off), t)

    def at_tp(off):
        return (k, partner(t, off))

    smalls = [
        (tokens_hbm, tokens_ref), (norm_gain_hbm, norm_gain_ref), (w_ig_hbm, w_ig_ref), (w_fg_hbm, w_fg_ref),
        (memory_max_hbm, memory_max_ref), (normalizer_hbm, normalizer_ref), (gain_hbm, gain_ref),
    ]
    smalls = [pltpu.make_async_copy(src, dst, small_sem.at[i]) for i, (src, dst) in enumerate(smalls)]
    smalls[0].start()
    peers = [at_tp(o) for o in range(1, nt)]
    peers += [at_plane(o) for o in range(1, ny)]
    peers += [at_zed(o) for o in range(1, nz)]
    barrier = pltpu.get_barrier_semaphore()
    for peer in peers:
        pl.semaphore_signal(barrier, inc=1, device_id=peer, device_id_type=MESH)

    pairs = [(w_query_hbm, w_query), (w_key_hbm, w_key), (w_value_hbm, w_value), (w_outgate_hbm, w_outgate)]
    pairs += [(memory_hbm.at[:, h], memory.at[:, h]) for h in range(heads)]
    pairs += [(w_out_hbm, w_out), (w_gate_hbm, w_gate), (w_up_hbm, w_up), (w_down_hbm, w_down)]
    loads = [pltpu.make_async_copy(src, dst, load_sem.at[i % DEPTH]) for i, (src, dst) in enumerate(pairs)]
    for load in smalls[1:] + loads[:DEPTH]:
        load.start()

    def arrived(i):
        loads[i].wait()
        if i + DEPTH < len(loads):
            loads[i + DEPTH].start()

    def push(src, dst, send_sem, recv_sem, device):
        pltpu.make_async_remote_copy(
            src_ref=src, dst_ref=dst, send_sem=send_sem, recv_sem=recv_sem,
            device_id=device, device_id_type=MESH,
        ).start()

    def drain(ref, sem):
        pltpu.make_async_copy(ref, ref, sem).wait()

    smalls[0].wait()
    pl.semaphore_wait(barrier, len(peers))
    for o in range(1, nt):
        push(tokens_ref, tok.at[o - 1], tok_sem.at[1], tok_sem.at[0], at_tp(o))
    total_in[z] = jnp.zeros((own, cols), BF16)
    for load in smalls[1:]:
        load.wait()
    if nt > 1:
        drain(tok, tok_sem.at[0])
    blocks = [(t, tokens_ref[...].astype(F32))]
    blocks += [(partner(t, o), tok[o - 1].astype(F32)) for o in range(1, nt)]
    square = jnp.sum(blocks[0][1] * blocks[0][1], axis=-1, keepdims=True)
    for _, block in blocks[1:]:
        square = square + jnp.sum(block * block, axis=-1, keepdims=True)
    row_scale = lax.rsqrt(square / width + 1e-06)
    for owner, block in blocks:
        at = pl.ds(pl.multiple_of(owner * cols, cols), cols)
        normed[:, at] = (block * row_scale * norm_gain_ref[:, at]).astype(BF16)
    x = normed[...]
    products = []
    for i, weight in enumerate([w_query, w_key, w_value, w_outgate]):
        arrived(i)
        products.append(jnp.dot(x, weight[...], preferred_element_type=F32))
    queries, keys, values, outgates = products
    queries = queries * dim ** (-0.5)
    igates, fgates = nt_dot(w_ig_ref[...], x), nt_dot(w_fg_ref[...], x)
    diagonal = lax.broadcasted_iota(jnp.int32, (own, own), 0) == lax.broadcasted_iota(jnp.int32, (own, own), 1)

    def along(row):
        return jnp.sum(jnp.where(diagonal, row, 0.0), axis=-1, keepdims=True)

    def mine(gates):
        picked = gates[0:heads]
        for i in range(1, nt):
            picked = jnp.where(t == i, gates[i * heads : (i + 1) * heads], picked)
        return picked

    igate, forget = mine(igates), mine(fgates)
    carried = jnp.minimum(forget, 0.0) - jnp.log1p(jnp.exp(-jnp.abs(forget))) + memory_max_ref[...]
    new_max = jnp.maximum(carried, igate)
    new_max_ref[...] = new_max
    keep_row, admit_row, floor_row = jnp.exp(carried - new_max), jnp.exp(igate - new_max), jnp.exp(-new_max)
    cut = [slice(h * dim, (h + 1) * dim) for h in range(heads)]
    first = 4
    for h in range(heads):
        arrived(first + h)
    for h in range(heads):
        turned = queries[:, cut[h]].T
        for r in range(own):
            num[h, r : r + 1, :] = jnp.sum(memory[r, h] * turned[:, r : r + 1], axis=0, keepdims=True)
    for h in range(heads):
        keep = jnp.broadcast_to(along(keep_row[h : h + 1]), (own, dim))
        key, value, query = along(admit_row[h : h + 1]) * keys[:, cut[h]], values[:, cut[h]], queries[:, cut[h]]
        factors[0, h], factors[1, h], factors[2, h] = keep, key, value
        grown = keep * normalizer_ref[:, h, :] + key
        new_norm[:, h, :] = grown
        denominator = jnp.sum(query * grown, axis=-1, keepdims=True)
        match = jnp.sum(query * key, axis=-1, keepdims=True)
        numerator = keep * num[h] + match * value
        cell_out = numerator / jnp.maximum(jnp.abs(denominator), along(floor_row[h : h + 1]))
        centered = cell_out - jnp.mean(cell_out, axis=-1, keepdims=True)
        head_var = jnp.mean(centered * centered, axis=-1, keepdims=True)
        gate = 1.0 / (1.0 + jnp.exp(-outgates[:, cut[h]]))
        mixed_ref[:, cut[h]] = (gate * centered * lax.rsqrt(head_var + 1e-05)).astype(BF16)

    for o in range(1, nt):
        push(mixed_ref, mix.at[o - 1], mix_sem.at[1], mix_sem.at[0], at_tp(o))
    first += heads
    arrived(first)
    inner = mixed_ref.shape[1]

    def project(value, owner):
        return jnp.dot(value, w_out[pl.ds(pl.multiple_of(owner * inner, inner), inner), :], preferred_element_type=F32)

    acc = tokens_ref[...].astype(F32) + project(mixed_ref[...], t)
    if nt > 1:
        drain(mix, mix_sem.at[0])
    for o in range(1, nt):
        acc = acc + project(mix[o - 1], partner(t, o))
    rows[k] = acc.astype(BF16)

    def spread(source, c):
        for o in range(1, ny):
            push(rows.at[source], rows.at[source], gather_send, plane_recv.at[c], at_plane(o))

    for o in reversed(range(1, nz)):
        push(rows.at[k], rows.at[k], gather_send, zed_recv.at[z], at_zed(o))
    spread(k, z)

    def forward(c):
        @pl.when(z != c)
        def _():
            drain(rows.at[c * ny + y], zed_recv.at[c])
            spread(c * ny + y, c)

    for c in range(nz):
        forward(c)
    for h in range(heads):
        turned = factors[1, h].T
        for r in range(own):
            memory[r, h] = factors[0, h, r : r + 1] * memory[r, h] + turned[:, r : r + 1] * factors[2, h, r : r + 1]

    gates = {}
    arrived(first + 1)
    arrived(first + 2)
    arrived(first + 3)

    def stage_a(c):
        if ny > 1:
            drain(rows.at[pl.ds(0, ny - 1)], plane_recv.at[c])
        xf = rows[c * ny : (c + 1) * ny].reshape(ny * own, cols).astype(F32)
        square = jnp.sum(xf * xf, axis=-1, keepdims=True)
        h = (xf * gain_ref[...]).astype(BF16)
        gate = nt_dot(h, w_gate[...])
        up = nt_dot(h, w_up[...])
        high = square.astype(BF16).astype(F32)
        lane = lax.broadcasted_iota(jnp.int32, (ny * own, 128), 1)
        part[c, :, 0:ff] = gate.astype(BF16)
        part[c, :, pad : pad + ff] = up.astype(BF16)
        part[c, :, 2 * pad :] = jnp.where(lane < 64, high, square - high).astype(BF16)
        for o in range(1, nt):
            push(part.at[c], part_in.at[c, o - 1], part_send, part_recv.at[c], at_tp(o))
        gates[c] = (gate, up, square)

    def stage_b(c):
        gate, up, square = gates.pop(c)
        if nt > 1:
            drain(part_in.at[c], part_recv.at[c])
        for o in range(1, nt):
            gate = gate + part_in[c, o - 1, :, 0:ff].astype(F32)
            up = up + part_in[c, o - 1, :, pad : pad + ff].astype(F32)
            tail = part_in[c, o - 1, :, 2 * pad :].astype(F32)
            square = square + jnp.sum(tail, axis=-1, keepdims=True) * (1.0 / 64)
        scale = lax.rsqrt(square / width + 1e-06)
        g = scale * gate
        hidden = (g / (1.0 + jnp.exp(-g)) * (scale * up)).astype(BF16)
        out = jnp.dot(hidden, w_down[...], preferred_element_type=F32)
        down[c] = out.reshape(ny, own, cols).astype(BF16)
        for o in range(1, ny):
            push(down.at[c, partner(y, o)], down_in.at[c, o - 1], reduce_send, down_recv.at[c], at_plane(o))

    def stage_c(c):
        acc = down[c, y].astype(F32)
        if ny > 1:
            drain(rows.at[pl.ds(0, ny - 1)], down_recv.at[c])
        for o in range(1, ny):
            acc = acc + down_in[c, o - 1].astype(F32)

        @pl.when(z == c)
        def _():
            ours[...] = acc

        @pl.when(z != c)
        def _():
            total[c] = acc.astype(BF16)
            push(total.at[c], total_in.at[z], reduce_send, total_recv, (c * ny + y, t))

    stage_a(0)
    for c in range(1, nz + 1):
        if c < nz:
            stage_a(c)
        stage_b(c - 1)
    for c in range(nz):
        stage_c(c)
    acc = rows[k].astype(F32) + ours[...]
    if nz > 1:
        drain(rows.at[pl.ds(0, nz - 1)], total_recv)
    for c in range(nz):
        acc = acc + total_in[c].astype(F32)
    out_ref[...] = acc.astype(BF16)
    if n > 1:
        drain(rows.at[pl.ds(0, n - 1)], gather_send)
        drain(rows.at[pl.ds(0, n - 1)], reduce_send)
    if nt > 1:
        drain(tok, tok_sem.at[1])
        drain(mix, mix_sem.at[1])
        drain(part_in, part_send)


def store_kernel(result, memory, normalizer, new_max, result_hbm, memory_hbm, normalizer_hbm, new_max_hbm, sem):
    pairs = [(memory, memory_hbm), (normalizer, normalizer_hbm), (new_max, new_max_hbm), (result, result_hbm)]
    copies = [pltpu.make_async_copy(src, dst, sem.at[i]) for i, (src, dst) in enumerate(pairs)]
    for copy in copies:
        copy.start()
    for copy in copies:
        copy.wait()


def per_device(
    mesh, tokens, norm_gain, w_query, w_key, w_value, w_outgate, w_input_gate, w_forget_gate,
    memory, normalizer, memory_max, w_output, ffn_gain, w_gate, w_up, w_down,
):
    n, nt = mesh.shape["kv"], mesh.shape["tp"]
    nz, ny = split_groups(n)
    own, cols = tokens.shape
    heads, dim = memory.shape[1], memory.shape[2]
    inner = heads * dim
    ff = w_down.shape[0]
    pad = -(-ff // 128) * 128
    dma = pltpu.SemaphoreType.DMA
    peers = max(nt - 1, 1)
    w_gate, w_up = w_gate.T, w_up.T
    vm = lambda like: pltpu.VMEM(like.shape, like.dtype)
    kept = 4 * (memory.size + 2 * normalizer.size) + 2 * tokens.size
    result, new_memory, new_normalizer, new_max = pl.pallas_call(
        functools.partial(step_kernel, nz, ny, nt, cols * nt),
        out_shape=(
            pltpu.VMEM((own, cols), BF16),
            pltpu.VMEM(memory.shape, F32),
            pltpu.VMEM(normalizer.shape, F32),
            pltpu.VMEM((heads, own), F32),
        ),
        in_specs=[HBM] * 16,
        out_specs=(VMEM,) * 4,
        scratch_shapes=[
            vm(tokens), pltpu.VMEM((1, cols * nt), F32), pltpu.VMEM(w_input_gate.shape[::-1], BF16),
            pltpu.VMEM(w_forget_gate.shape[::-1], BF16), vm(normalizer), pltpu.VMEM((heads, own), F32),
            pltpu.VMEM((1, cols), F32),
            vm(w_key), vm(w_value), vm(w_query), vm(w_outgate),
            vm(w_output), vm(w_gate), vm(w_up), vm(w_down),
            pltpu.VMEM((peers, own, cols), BF16),
            pltpu.VMEM((own, cols * nt), BF16),
            pltpu.VMEM((heads, own, dim), F32),
            pltpu.VMEM((3, heads, own, dim), F32),
            pltpu.VMEM((own, inner), BF16),
            pltpu.VMEM((peers, own, inner), BF16),
            pltpu.VMEM((n, own, cols), BF16),
            pltpu.VMEM((nz, ny * own, 2 * pad + 128), BF16),
            pltpu.VMEM((nz, peers, ny * own, 2 * pad + 128), BF16),
            pltpu.VMEM((nz, ny, own, cols), BF16),
            pltpu.VMEM((nz, max(ny - 1, 1), own, cols), BF16),
            pltpu.VMEM((nz, own, cols), BF16),
            pltpu.VMEM((nz, own, cols), BF16),
            pltpu.VMEM((own, cols), F32),
            dma((7,)),
            dma((DEPTH,)),
            dma((2,)),
            dma((2,)),
            dma((nz,)),
            dma((nz,)),
            dma,
            dma((nz,)),
            dma,
            dma((nz,)),
            dma,
            dma,
        ],
        compiler_params=pltpu.CompilerParams(collective_id=0, has_side_effects=True, vmem_limit_bytes=VMEM_BYTES - kept),
        name="decode_step",
    )(
        tokens, norm_gain.reshape(1, -1), w_input_gate.T, w_forget_gate.T, normalizer, memory_max.T,
        ffn_gain.reshape(1, cols), w_key, w_value, w_query, w_outgate, memory, w_output, w_gate, w_up, w_down,
    )
    result, new_memory, new_normalizer, new_max = pl.pallas_call(
        store_kernel,
        out_shape=(
            jax.ShapeDtypeStruct(tokens.shape, BF16),
            jax.ShapeDtypeStruct(memory.shape, F32),
            jax.ShapeDtypeStruct(normalizer.shape, F32),
            jax.ShapeDtypeStruct((heads, own), F32),
        ),
        in_specs=[VMEM] * 4,
        out_specs=(HBM,) * 4,
        scratch_shapes=[dma((4,))],
        compiler_params=pltpu.CompilerParams(vmem_limit_bytes=2**20),
        name="store",
    )(result, new_memory, new_normalizer, new_max)
    return (result, new_memory, new_normalizer, new_max.T)


def solution(mesh):
    placed = (
        P("kv", "tp"),
        P(),
        P(None, "tp"),
        P(None, "tp"),
        P(None, "tp"),
        P(None, "tp"),
        P(),
        P(),
        P("kv", "tp", None, None),
        P("kv", "tp", None),
        P("kv", "tp"),
        P(None, "tp"),
        P("tp"),
        P("tp", "kv"),
        P("tp", "kv"),
        P("kv", "tp"),
    )
    return jax.shard_map(
        functools.partial(per_device, mesh),
        mesh=mesh,
        in_specs=placed,
        out_specs=(P("kv", "tp"), P("kv", "tp", None, None), P("kv", "tp", None), P("kv", "tp")),
        check_vma=False,
    )
```

time: 42 us -> 33.7 us (0.80)
  Pallas kernels: 41.2 us -> 32.9 us
    pallas_call x1, Pallas kernels: 36 us -> 30.9 us  [per_device(): pl.pallas_call(functools.partial(step_kernel, nz, ny, nt, cols * nt), out...]
    pallas_call x1, Pallas kernels: 5.2 us -> 2.06 us  [per_device(): pl.pallas_call(store_kernel, out_shape=(jax.ShapeDtypeStruct(tokens.shape...]
where the time goes in v1:
time: 33.7 us; the launch traced here: 33.6 us
  Pallas kernels  32.9 us (98%)
  between operations  0.65 us (2%)
    pallas_call x1, Pallas kernels, per_device(): pl.pallas_call(functools.partial(step_kernel, nz, ny, nt, cols * nt), out...  30.9 us
    pallas_call x1, Pallas kernels, per_device(): pl.pallas_call(store_kernel, out_shape=(jax.ShapeDtypeStruct(tokens.shape...  2.06 us

profile of v1, /device:TPU:0, one launch (start us, length us, event | category | flops | bytes accessed | tf_op | source)
XLA Modules:
  0.0 33.6 jit_solution(1283433290477075236)
XLA Ops:
  0.6 30.9 %decode_step.1 = (bf16[16,1024]{1,0:T(8,128)(2,1)S(1)}, f32[16,4,128,128]{3,2,1,0:T(8,128)S(1)}, f32[16,4,128]{2,1,0:T(4,128)S(1)}, f32[4,16]{1,0:T(4,128)S(1)}) custom-call(bf16[16,1024]{1,0:T(8,128)(2,1)} %tokens_hbm.1, f32[1,2048]{1,0:T(1,128)} %bitcast.12, bf16[8,2048]{1,0:T(8,128)(2,1)} %bitcast.10, bf16[8,2048]{1,0:T(8,128)(2,1)} %bitcast.11, ...), custom_call_target="tpu_custom_call" | custom-call | tf_op jit(solution)/shard_map/decode_step/pallas_call | solution.py:305
  31.5 2.1 %store.1 = (bf16[16,1024]{1,0:T(8,128)(2,1)}, f32[16,4,128,128]{3,2,1,0:T(8,128)}, f32[16,4,128]{2,1,0:T(4,128)}, f32[4,16]{1,0:T(4,128)}) custom-call(bf16[16,1024]{1,0:T(8,128)(2,1)S(1)} %get-tuple-element.12.result, f32[16,4,128,128]{3,2,1,0:T(8,128)S(1)} %get-tuple-element.13.memory, f32[16,4,128]{2,1,0:T(4,128)S(1)} %get-tuple-element.14.normalizer, ...), custom_call_target="tpu_custom_call" | custom-call | tf_op jit(solution)/shard_map/store/pallas_call | solution.py:354

commit v2 on v1

--- a/solution.py
+++ b/solution.py
@@ -12,7 +12,7 @@
 ANY = pl.BlockSpec(memory_space=pl.ANY)
 VMEM = pl.BlockSpec(memory_space=pltpu.VMEM)
 HBM = pl.BlockSpec(memory_space=pltpu.HBM)
-DEPTH = 6
+DEPTH = 8
 VMEM_BYTES = 67043328
 
 
@@ -46,7 +46,7 @@
     w_key, w_value, w_query, w_outgate, w_out, w_gate, w_up, w_down,
     tok, normed, num, factors, mixed_ref, mix, rows, part, part_in, down, down_in, total, total_in, ours,
     small_sem, load_sem, tok_sem, mix_sem, zed_recv, plane_recv, gather_send,
-    part_recv, part_send, down_recv, total_recv, reduce_send,
+    part_recv, part_send, down_recv, total_recv, reduce_send, ahead_sem, behind_sem,
 ):
     k, t = lax.axis_index("kv"), lax.axis_index("tp")
     z, y = k // ny, k % ny
@@ -54,9 +54,7 @@
     heads, dim = memory.shape[1], memory.shape[3]
     ff = w_down.shape[0]
     pad = (part.shape[2] - 128) // 2
-
-    def at_zed(off):
-        return (partner(z, off) * ny + y, t)
+    plane_order = sorted(range(1, ny), key=lambda o: -bin(o).count("1"))
 
     def at_plane(off):
         return (z * ny + partner(y, off), t)
@@ -70,18 +68,39 @@
     ]
     smalls = [pltpu.make_async_copy(src, dst, small_sem.at[i]) for i, (src, dst) in enumerate(smalls)]
     smalls[0].start()
+    smalls[1].start()
     peers = [at_tp(o) for o in range(1, nt)]
     peers += [at_plane(o) for o in range(1, ny)]
-    peers += [at_zed(o) for o in range(1, nz)]
     barrier = pltpu.get_barrier_semaphore()
+
+    def at_step(d):
+        return ((z + d) * ny + y, t)
+
+    def greet(sem, device):
+        pl.semaphore_signal(sem, inc=1, device_id=device, device_id_type=MESH)
+
     for peer in peers:
-        pl.semaphore_signal(barrier, inc=1, device_id=peer, device_id_type=MESH)
-
-    pairs = [(w_query_hbm, w_query), (w_key_hbm, w_key), (w_value_hbm, w_value), (w_outgate_hbm, w_outgate)]
+        greet(barrier, peer)
+    if nz > 1:
+        pl.when(z + 1 < nz)(lambda: greet(barrier, at_step(1)))
+        pl.when(z >= 1)(lambda: greet(barrier, at_step(-1)))
+
+    def tell(d):
+        pl.when((z >= 1) & (z + d < nz))(lambda: greet(ahead_sem.at[d + 1], at_step(-1)))
+        pl.when((z + 1 < nz) & (z >= d))(lambda: greet(behind_sem.at[d + 1], at_step(1)))
+
+    def hear(d):
+        pl.when(z + d < nz)(lambda: pl.semaphore_wait(ahead_sem.at[d], 1))
+        pl.when(z >= d)(lambda: pl.semaphore_wait(behind_sem.at[d], 1))
+        if d + 1 < nz:
+            tell(d)
+
+    pairs = [(w_query_hbm, w_query)]
     pairs += [(memory_hbm.at[:, h], memory.at[:, h]) for h in range(heads)]
+    pairs += [(w_key_hbm, w_key), (w_value_hbm, w_value), (w_outgate_hbm, w_outgate)]
     pairs += [(w_out_hbm, w_out), (w_gate_hbm, w_gate), (w_up_hbm, w_up), (w_down_hbm, w_down)]
     loads = [pltpu.make_async_copy(src, dst, load_sem.at[i % DEPTH]) for i, (src, dst) in enumerate(pairs)]
-    for load in smalls[1:] + loads[:DEPTH]:
+    for load in loads[:1] + smalls[2:] + loads[1:DEPTH]:
         load.start()
 
     def arrived(i):
@@ -99,12 +118,13 @@
         pltpu.make_async_copy(ref, ref, sem).wait()
 
     smalls[0].wait()
-    pl.semaphore_wait(barrier, len(peers))
+    pl.semaphore_wait(barrier, len(peers) + (2 * nz - 2 - z) // nz + (z + nz - 1) // nz)
     for o in range(1, nt):
         push(tokens_ref, tok.at[o - 1], tok_sem.at[1], tok_sem.at[0], at_tp(o))
+    if nz > 2:
+        tell(1)
     total_in[z] = jnp.zeros((own, cols), BF16)
-    for load in smalls[1:]:
-        load.wait()
+    smalls[1].wait()
     if nt > 1:
         drain(tok, tok_sem.at[0])
     blocks = [(t, tokens_ref[...].astype(F32))]
@@ -117,12 +137,33 @@
         at = pl.ds(pl.multiple_of(owner * cols, cols), cols)
         normed[:, at] = (block * row_scale * norm_gain_ref[:, at]).astype(BF16)
     x = normed[...]
-    products = []
-    for i, weight in enumerate([w_query, w_key, w_value, w_outgate]):
+    cut = [slice(h * dim, (h + 1) * dim) for h in range(heads)]
+
+    def projected(i, weight):
         arrived(i)
-        products.append(jnp.dot(x, weight[...], preferred_element_type=F32))
-    queries, keys, values, outgates = products
-    queries = queries * dim ** (-0.5)
+        return jnp.dot(x, weight[...], preferred_element_type=F32)
+
+    def recall(some):
+        for h in some:
+            turned = queries[:, cut[h]].T
+            for r in range(own):
+                num[h, r : r + 1, :] = jnp.sum(memory[r, h] * turned[:, r : r + 1], axis=0, keepdims=True)
+
+    queries = projected(0, w_query) * dim ** (-0.5)
+    for h in range(heads):
+        arrived(1 + h)
+    first = 1 + heads
+    third = -(-heads // 3)
+    keys = projected(first, w_key)
+    recall(range(heads)[:third])
+    values = projected(first + 1, w_value)
+    recall(range(heads)[third : heads - heads // 3])
+    if nz > 2:
+        hear(2)
+    for load in smalls[2:]:
+        load.wait()
+    outgates = projected(first + 2, w_outgate)
+    recall(range(heads)[heads - heads // 3 :])
     igates, fgates = nt_dot(w_ig_ref[...], x), nt_dot(w_fg_ref[...], x)
     diagonal = lax.broadcasted_iota(jnp.int32, (own, own), 0) == lax.broadcasted_iota(jnp.int32, (own, own), 1)
 
@@ -140,14 +181,6 @@
     new_max = jnp.maximum(carried, igate)
     new_max_ref[...] = new_max
     keep_row, admit_row, floor_row = jnp.exp(carried - new_max), jnp.exp(igate - new_max), jnp.exp(-new_max)
-    cut = [slice(h * dim, (h + 1) * dim) for h in range(heads)]
-    first = 4
-    for h in range(heads):
-        arrived(first + h)
-    for h in range(heads):
-        turned = queries[:, cut[h]].T
-        for r in range(own):
-            num[h, r : r + 1, :] = jnp.sum(memory[r, h] * turned[:, r : r + 1], axis=0, keepdims=True)
     for h in range(heads):
         keep = jnp.broadcast_to(along(keep_row[h : h + 1]), (own, dim))
         key, value, query = along(admit_row[h : h + 1]) * keys[:, cut[h]], values[:, cut[h]], queries[:, cut[h]]
@@ -165,7 +198,7 @@
 
     for o in range(1, nt):
         push(mixed_ref, mix.at[o - 1], mix_sem.at[1], mix_sem.at[0], at_tp(o))
-    first += heads
+    first += 3
     arrived(first)
     inner = mixed_ref.shape[1]
 
@@ -180,26 +213,32 @@
     rows[k] = acc.astype(BF16)
 
     def spread(source, c):
-        for o in range(1, ny):
+        for o in plane_order:
             push(rows.at[source], rows.at[source], gather_send, plane_recv.at[c], at_plane(o))
 
-    for o in reversed(range(1, nz)):
-        push(rows.at[k], rows.at[k], gather_send, zed_recv.at[z], at_zed(o))
+    for d in range(3, nz):
+        hear(d)
+
+    def offer(c):
+        push(rows.at[k], rows.at[k], gather_send, zed_recv.at[z], (c * ny + y, t))
+
+    for d in reversed(range(1, nz)):
+        pl.when(z + d < nz)(functools.partial(offer, z + d))
+        pl.when(z >= d)(functools.partial(offer, z - d))
     spread(k, z)
-
-    def forward(c):
-        @pl.when(z != c)
-        def _():
-            drain(rows.at[c * ny + y], zed_recv.at[c])
-            spread(c * ny + y, c)
-
-    for c in range(nz):
-        forward(c)
     for h in range(heads):
         turned = factors[1, h].T
         for r in range(own):
             memory[r, h] = factors[0, h, r : r + 1] * memory[r, h] + turned[:, r : r + 1] * factors[2, h, r : r + 1]
 
+    def chunk(j):
+        return j - 1 + (nz + j - 1 - z) // nz if j else z
+
+    def forward(j):
+        c = chunk(j)
+        drain(rows.at[c * ny + y], zed_recv.at[c])
+        spread(c * ny + y, c)
+
     gates = {}
     arrived(first + 1)
     arrived(first + 2)
@@ -207,8 +246,8 @@
 
     def stage_a(c):
         if ny > 1:
-            drain(rows.at[pl.ds(0, ny - 1)], plane_recv.at[c])
-        xf = rows[c * ny : (c + 1) * ny].reshape(ny * own, cols).astype(F32)
+            drain(rows.at[pl.ds(0, ny - 1)], plane_recv.at[chunk(c)])
+        xf = rows[pl.ds(chunk(c) * ny, ny)].reshape(ny * own, cols).astype(F32)
         square = jnp.sum(xf * xf, axis=-1, keepdims=True)
         h = (xf * gain_ref[...]).astype(BF16)
         gate = nt_dot(h, w_gate[...])
@@ -236,7 +275,7 @@
         hidden = (g / (1.0 + jnp.exp(-g)) * (scale * up)).astype(BF16)
         out = jnp.dot(hidden, w_down[...], preferred_element_type=F32)
         down[c] = out.reshape(ny, own, cols).astype(BF16)
-        for o in range(1, ny):
+        for o in plane_order:
             push(down.at[c, partner(y, o)], down_in.at[c, o - 1], reduce_send, down_recv.at[c], at_plane(o))
 
     def stage_c(c):
@@ -246,22 +285,26 @@
         for o in range(1, ny):
             acc = acc + down_in[c, o - 1].astype(F32)
 
-        @pl.when(z == c)
-        def _():
+        if c == 0:
             ours[...] = acc
-
-        @pl.when(z != c)
-        def _():
+        else:
             total[c] = acc.astype(BF16)
-            push(total.at[c], total_in.at[z], reduce_send, total_recv, (c * ny + y, t))
-
+            push(total.at[c], total_in.at[z], reduce_send, total_recv, (chunk(c) * ny + y, t))
+
+    if nz > 1:
+        forward(1)
     stage_a(0)
-    for c in range(1, nz + 1):
-        if c < nz:
-            stage_a(c)
-        stage_b(c - 1)
-    for c in range(nz):
-        stage_c(c)
+    for j in range(2, nz):
+        forward(j)
+    stage_b(0)
+    for j in range(1, nz + 1):
+        if j < nz:
+            stage_a(j)
+        if j > 1:
+            stage_b(j - 1)
+    for j in range(1, nz):
+        stage_c(j)
+    stage_c(0)
     acc = rows[k].astype(F32) + ours[...]
     if nz > 1:
         drain(rows.at[pl.ds(0, nz - 1)], total_recv)
@@ -344,6 +387,8 @@
             dma((nz,)),
             dma,
             dma,
+            pltpu.SemaphoreType.REGULAR((nz,)),
+            pltpu.SemaphoreType.REGULAR((nz,)),
         ],
         compiler_params=pltpu.CompilerParams(collective_id=0, has_side_effects=True, vmem_limit_bytes=VMEM_BYTES - kept),
         name="decode_step",

time: 33.7 us -> 30.7 us (0.911)
  Pallas kernels: 32.9 us -> 29.9 us
    pallas_call x1, Pallas kernels: 30.9 us -> 27.9 us  [per_device(): pl.pallas_call(functools.partial(step_kernel, nz, ny, nt, cols * nt), out...]
where the time goes in v2:
time: 30.7 us; the launch traced here: 30.6 us
  Pallas kernels  29.9 us (97%)
  between operations  0.65 us (2%)
    pallas_call x1, Pallas kernels, per_device(): pl.pallas_call(functools.partial(step_kernel, nz, ny, nt, cols * nt), out...  27.9 us
    pallas_call x1, Pallas kernels, per_device(): pl.pallas_call(store_kernel, out_shape=(jax.ShapeDtypeStruct(tokens.shape...  2.06 us

profile of v2, /device:TPU:0, one launch (start us, length us, event | category | flops | bytes accessed | tf_op | source)
XLA Modules:
  0.0 30.6 jit_solution(9257624860555752492)
XLA Ops:
  0.6 27.9 %decode_step.1 = (bf16[16,1024]{1,0:T(8,128)(2,1)S(1)}, f32[16,4,128,128]{3,2,1,0:T(8,128)S(1)}, f32[16,4,128]{2,1,0:T(4,128)S(1)}, f32[4,16]{1,0:T(4,128)S(1)}) custom-call(bf16[16,1024]{1,0:T(8,128)(2,1)} %tokens_hbm.1, f32[1,2048]{1,0:T(1,128)} %bitcast.12, bf16[8,2048]{1,0:T(8,128)(2,1)} %bitcast.10, bf16[8,2048]{1,0:T(8,128)(2,1)} %bitcast.11, ...), custom_call_target="tpu_custom_call" | custom-call | tf_op jit(solution)/shard_map/decode_step/pallas_call | solution.py:348
  28.5 2.1 %store.1 = (bf16[16,1024]{1,0:T(8,128)(2,1)}, f32[16,4,128,128]{3,2,1,0:T(8,128)}, f32[16,4,128]{2,1,0:T(4,128)}, f32[4,16]{1,0:T(4,128)}) custom-call(bf16[16,1024]{1,0:T(8,128)(2,1)S(1)} %get-tuple-element.12.result, f32[16,4,128,128]{3,2,1,0:T(8,128)S(1)} %get-tuple-element.13.memory, f32[16,4,128]{2,1,0:T(4,128)S(1)} %get-tuple-element.14.normalizer, ...), custom_call_target="tpu_custom_call" | custom-call | tf_op jit(solution)/shard_map/store/pallas_call | solution.py:399

commit v3 on v2

--- a/solution.py
+++ b/solution.py
@@ -31,6 +31,12 @@
         slow *= 2
     assert count % slow == 0
     return slow, count // slow
+
+
+def parts_of(width, count):
+    count = max(1, min(count, width // 128))
+    step = width // count
+    return [slice(i * step, (i + 1) * step) for i in range(count)]
 
 
 def nt_dot(a, b):
@@ -54,6 +60,7 @@
     heads, dim = memory.shape[1], memory.shape[3]
     ff = w_down.shape[0]
     pad = (part.shape[2] - 128) // 2
+    gather_parts, reduce_parts = parts_of(cols, 2), parts_of(cols, 2)
     plane_order = sorted(range(1, ny), key=lambda o: -bin(o).count("1"))
 
     def at_plane(off):
@@ -212,19 +219,22 @@
         acc = acc + project(mix[o - 1], partner(t, o))
     rows[k] = acc.astype(BF16)
 
-    def spread(source, c):
+    def spread(source, c, piece=slice(None)):
         for o in plane_order:
-            push(rows.at[source], rows.at[source], gather_send, plane_recv.at[c], at_plane(o))
+            ref = rows.at[source, :, piece]
+            push(ref, ref, gather_send, plane_recv.at[c], at_plane(o))
 
     for d in range(3, nz):
         hear(d)
 
-    def offer(c):
-        push(rows.at[k], rows.at[k], gather_send, zed_recv.at[z], (c * ny + y, t))
-
-    for d in reversed(range(1, nz)):
-        pl.when(z + d < nz)(functools.partial(offer, z + d))
-        pl.when(z >= d)(functools.partial(offer, z - d))
+    def offer(i, c):
+        ref = rows.at[k, :, gather_parts[i]]
+        push(ref, ref, gather_send, zed_recv.at[i, z], (c * ny + y, t))
+
+    for i in range(len(gather_parts)):
+        for d in reversed(range(1, nz)):
+            pl.when(z + d < nz)(functools.partial(offer, i, z + d))
+            pl.when(z >= d)(functools.partial(offer, i, z - d))
     spread(k, z)
     for h in range(heads):
         turned = factors[1, h].T
@@ -236,8 +246,9 @@
 
     def forward(j):
         c = chunk(j)
-        drain(rows.at[c * ny + y], zed_recv.at[c])
-        spread(c * ny + y, c)
+        for i, piece in enumerate(gather_parts):
+            drain(rows.at[c * ny + y, :, piece], zed_recv.at[i, c])
+            spread(c * ny + y, c, piece)
 
     gates = {}
     arrived(first + 1)
@@ -275,21 +286,24 @@
         hidden = (g / (1.0 + jnp.exp(-g)) * (scale * up)).astype(BF16)
         out = jnp.dot(hidden, w_down[...], preferred_element_type=F32)
         down[c] = out.reshape(ny, own, cols).astype(BF16)
-        for o in plane_order:
-            push(down.at[c, partner(y, o)], down_in.at[c, o - 1], reduce_send, down_recv.at[c], at_plane(o))
+        for i, piece in enumerate(reduce_parts):
+            for o in plane_order:
+                src, dst = down.at[c, partner(y, o), :, piece], down_in.at[c, o - 1, :, piece]
+                push(src, dst, reduce_send, down_recv.at[i, c], at_plane(o))
 
     def stage_c(c):
-        acc = down[c, y].astype(F32)
-        if ny > 1:
-            drain(rows.at[pl.ds(0, ny - 1)], down_recv.at[c])
-        for o in range(1, ny):
-            acc = acc + down_in[c, o - 1].astype(F32)
-
-        if c == 0:
-            ours[...] = acc
-        else:
-            total[c] = acc.astype(BF16)
-            push(total.at[c], total_in.at[z], reduce_send, total_recv, (chunk(c) * ny + y, t))
+        for i, piece in enumerate(reduce_parts):
+            acc = down[c, y, :, piece].astype(F32)
+            if ny > 1:
+                drain(rows.at[pl.ds(0, ny - 1), :, piece], down_recv.at[i, c])
+            for o in range(1, ny):
+                acc = acc + down_in[c, o - 1, :, piece].astype(F32)
+            if c == 0:
+                ours[:, piece] = acc
+            else:
+                total[c, :, piece] = acc.astype(BF16)
+                src, dst = total.at[c, :, piece], total_in.at[z, :, piece]
+                push(src, dst, reduce_send, total_recv, (chunk(c) * ny + y, t))
 
     if nz > 1:
         forward(1)
@@ -297,10 +311,13 @@
     for j in range(2, nz):
         forward(j)
     stage_b(0)
-    for j in range(1, nz + 1):
+    if nz > 1:
+        stage_a(1)
+        stage_b(1)
+    for j in range(2, nz + 1):
         if j < nz:
             stage_a(j)
-        if j > 1:
+        if j > 2:
             stage_b(j - 1)
     for j in range(1, nz):
         stage_c(j)
@@ -379,12 +396,12 @@
             dma((DEPTH,)),
             dma((2,)),
             dma((2,)),
-            dma((nz,)),
+            dma((2, nz)),
             dma((nz,)),
             dma,
             dma((nz,)),
             dma,
-            dma((nz,)),
+            dma((2, nz)),
             dma,
             dma,
             pltpu.SemaphoreType.REGULAR((nz,)),

time: 30.7 us -> 29.8 us (0.971)
  Pallas kernels: 29.9 us -> 29 us
    pallas_call x1, Pallas kernels: 27.9 us -> 27 us  [per_device(): pl.pallas_call(functools.partial(step_kernel, nz, ny, nt, cols * nt), out...]
where the time goes in v3:
time: 29.8 us; the launch traced here: 29.7 us
  Pallas kernels  29 us (97%)
  between operations  0.65 us (2%)
    pallas_call x1, Pallas kernels, per_device(): pl.pallas_call(functools.partial(step_kernel, nz, ny, nt, cols * nt), out...  27 us
    pallas_call x1, Pallas kernels, per_device(): pl.pallas_call(store_kernel, out_shape=(jax.ShapeDtypeStruct(tokens.shape...  2.06 us

profile of v3, /device:TPU:0, one launch (start us, length us, event | category | flops | bytes accessed | tf_op | source)
XLA Modules:
  0.0 29.7 jit_solution(2942080364626250932)
XLA Ops:
  0.6 27.0 %decode_step.1 = (bf16[16,1024]{1,0:T(8,128)(2,1)S(1)}, f32[16,4,128,128]{3,2,1,0:T(8,128)S(1)}, f32[16,4,128]{2,1,0:T(4,128)S(1)}, f32[4,16]{1,0:T(4,128)S(1)}) custom-call(bf16[16,1024]{1,0:T(8,128)(2,1)} %tokens_hbm.1, f32[1,2048]{1,0:T(1,128)} %bitcast.12, bf16[8,2048]{1,0:T(8,128)(2,1)} %bitcast.10, bf16[8,2048]{1,0:T(8,128)(2,1)} %bitcast.11, ...), custom_call_target="tpu_custom_call" | custom-call | tf_op jit(solution)/shard_map/decode_step/pallas_call | solution.py:365
  27.6 2.1 %store.1 = (bf16[16,1024]{1,0:T(8,128)(2,1)}, f32[16,4,128,128]{3,2,1,0:T(8,128)}, f32[16,4,128]{2,1,0:T(4,128)}, f32[4,16]{1,0:T(4,128)}) custom-call(bf16[16,1024]{1,0:T(8,128)(2,1)S(1)} %get-tuple-element.12.result, f32[16,4,128,128]{3,2,1,0:T(8,128)S(1)} %get-tuple-element.13.memory, f32[16,4,128]{2,1,0:T(4,128)S(1)} %get-tuple-element.14.normalizer, ...), custom_call_target="tpu_custom_call" | custom-call | tf_op jit(solution)/shard_map/store/pallas_call | solution.py:416

commit v4 on v3

--- a/solution.py
+++ b/solution.py
@@ -255,6 +255,10 @@
     arrived(first + 2)
     arrived(first + 3)
 
+    def share(c, span):
+        for o in range(1, nt):
+            push(part.at[c, :, span], part_in.at[c, o - 1, :, span], part_send, part_recv.at[c], at_tp(o))
+
     def stage_a(c):
         if ny > 1:
             drain(rows.at[pl.ds(0, ny - 1)], plane_recv.at[chunk(c)])
@@ -262,14 +266,14 @@
         square = jnp.sum(xf * xf, axis=-1, keepdims=True)
         h = (xf * gain_ref[...]).astype(BF16)
         gate = nt_dot(h, w_gate[...])
+        part[c, :, 0:ff] = gate.astype(BF16)
+        share(c, slice(0, pad))
         up = nt_dot(h, w_up[...])
         high = square.astype(BF16).astype(F32)
         lane = lax.broadcasted_iota(jnp.int32, (ny * own, 128), 1)
-        part[c, :, 0:ff] = gate.astype(BF16)
         part[c, :, pad : pad + ff] = up.astype(BF16)
         part[c, :, 2 * pad :] = jnp.where(lane < 64, high, square - high).astype(BF16)
-        for o in range(1, nt):
-            push(part.at[c], part_in.at[c, o - 1], part_send, part_recv.at[c], at_tp(o))
+        share(c, slice(pad, 2 * pad + 128))
         gates[c] = (gate, up, square)
 
     def stage_b(c):

time: 29.8 us -> 30.4 us (1.020); the launches traced: 29.7 us -> 30 us
  no operation moved by 1% of the time
where the time goes in v4:
time: 30.4 us; the launch traced here: 30 us
  Pallas kernels  29.3 us (96%)
  between operations  0.65 us (2%)
    pallas_call x1, Pallas kernels, per_device(): pl.pallas_call(functools.partial(step_kernel, nz, ny, nt, cols * nt), out...  27.3 us
    pallas_call x1, Pallas kernels, per_device(): pl.pallas_call(store_kernel, out_shape=(jax.ShapeDtypeStruct(tokens.shape...  2.06 us

profile of v4, /device:TPU:0, one launch (start us, length us, event | category | flops | bytes accessed | tf_op | source)
XLA Modules:
  0.0 30.0 jit_solution(15801784988264248881)
XLA Ops:
  0.6 27.3 %decode_step.1 = (bf16[16,1024]{1,0:T(8,128)(2,1)S(1)}, f32[16,4,128,128]{3,2,1,0:T(8,128)S(1)}, f32[16,4,128]{2,1,0:T(4,128)S(1)}, f32[4,16]{1,0:T(4,128)S(1)}) custom-call(bf16[16,1024]{1,0:T(8,128)(2,1)} %tokens_hbm.1, f32[1,2048]{1,0:T(1,128)} %bitcast.12, bf16[8,2048]{1,0:T(8,128)(2,1)} %bitcast.10, bf16[8,2048]{1,0:T(8,128)(2,1)} %bitcast.11, ...), custom_call_target="tpu_custom_call" | custom-call | tf_op jit(solution)/shard_map/decode_step/pallas_call | solution.py:369
  27.9 2.1 %store.1 = (bf16[16,1024]{1,0:T(8,128)(2,1)}, f32[16,4,128,128]{3,2,1,0:T(8,128)}, f32[16,4,128]{2,1,0:T(4,128)}, f32[4,16]{1,0:T(4,128)}) custom-call(bf16[16,1024]{1,0:T(8,128)(2,1)S(1)} %get-tuple-element.12.result, f32[16,4,128,128]{3,2,1,0:T(8,128)S(1)} %get-tuple-element.13.memory, f32[16,4,128]{2,1,0:T(4,128)S(1)} %get-tuple-element.14.normalizer, ...), custom_call_target="tpu_custom_call" | custom-call | tf_op jit(solution)/shard_map/store/pallas_call | solution.py:420
